TPU v7x, 1024 devices: a whole 4x8x16 slice. The times are simulated.
1024 devices in a mesh: sp: 16 (over z), tp: 64 (over y, x, core).
Axes of the slice: x: 4, y: 8, z: 16, core: 2. Of those that a mesh axis runs over, the one named last changes fastest.
Arguments:
- latent: bfloat16 [12288, 4096], P('sp', 'tp'), may hold values from -600 to 600
- context: bfloat16 [512, 4096], P('sp', 'tp'), may hold values from -600 to 600
- cond: float32 [4096], P('sp'), may hold values from -6 to 6
- ctx_cond: float32 [4096], P('sp'), may hold values from -6 to 6
- w_shift: bfloat16 [4096, 4096], P('sp', 'tp'), may hold values from -0.09375 to 0.09375
- w_scale: bfloat16 [4096, 4096], P('sp', 'tp'), may hold values from -0.09375 to 0.09375
- w_gate: bfloat16 [4096, 4096], P('sp', 'tp'), may hold values from -0.1875 to 0.1875
- norm_gain: float32 [4096], P('tp'), may hold values from 0.1 to 1.9
- w_query: bfloat16 [2048, 4096], P('tp'), may hold values from -0.09375 to 0.09375
- w_key: bfloat16 [2048, 4096], P('tp'), may hold values from -0.09375 to 0.09375
- w_value: bfloat16 [4096, 4096], P('tp'), may hold values from -0.09375 to 0.09375
- w_decay_fwd: bfloat16 [2048, 4096], P('tp'), may hold values from -0.09375 to 0.09375
- w_decay_bwd: bfloat16 [2048, 4096], P('tp'), may hold values from -0.09375 to 0.09375
- forgetting_shift_vector: float32 [2048], P('tp')
- decay_log: float32 [12288, 64], P('sp', 'tp'), may hold values from -3 to 0
- head_gain: float32 [4096], P('tp'), may hold values from 0.1 to 1.9
- w_out: bfloat16 [4096, 4096], P('tp'), may hold values from -0.09375 to 0.09375
Outputs:
- update: bfloat16 [12288, 4096], P('sp', 'tp')
All inputs are finite; a program needn't handle non-finite values.
Results may differ from a plain program's by a relative error of at most 0.012.
The roundings to bfloat16 on the way count: a program that leaves them out, or rounds other values in their place, can miss the bound.
Values may be sent and summed in bfloat16 or wider, within the bound.
A program may use at most 32 MiB of HBM per device.

v0:
```python
import jax
import jax.numpy as jnp
from jax import lax
from jax.sharding import PartitionSpec as P

WIDTH = 4096
ADDRESS_WIDTH = 32
VALUE_DIM = 64
BLOCK = 64


epsilon = 1e-06
smoothing_scale_factor = 16.0
highest_precision = lax.Precision.HIGHEST


def from_everyone(shard, axis):
    count = lax.axis_size(axis)
    return lax.all_to_all(
        jnp.broadcast_to(shard[None], (count, *shard.shape)), axis, 0, 0, tiled=True
    )


def taken_together(shard, axis):
    everything = from_everyone(shard, axis)
    return jnp.sum(everything, axis=0)


def together(arrays, axis):
    vector, at, gathered = (jnp.concatenate([a.reshape(-1) for a in arrays]), 0, [])
    so_far = taken_together(vector, axis)
    for a in arrays:
        gathered.append(so_far[at : at + a.size].reshape(a.shape))
        at += a.size
    return tuple(gathered)


def gather_turned(arrays, axis, dims):
    turned = [jnp.moveaxis(a, dim, 0) for a, dim in zip(arrays, dims)]
    both = jnp.concatenate([t.reshape(len(t), -1) for t in turned], axis=1)
    out, at, gathered = (lax.all_gather(both, axis, axis=0, tiled=True), 0, [])
    for t, dim in zip(turned, dims):
        slab = out[:, at : at + t[0].size].reshape(-1, *t.shape[1:])
        gathered.append(jnp.moveaxis(slab, 0, dim))
        at += t[0].size
    return tuple(gathered)


def in_one_piece(arrays, axis, dim, along):
    columns = [a.reshape(*a.shape[:along], -1) for a in arrays]
    both = jnp.concatenate(columns, axis=along)
    out, at, gathered = (lax.all_gather(both, axis, axis=dim, tiled=True), 0, [])
    for a, column in zip(arrays, columns):
        slab = out[..., at : at + column.shape[along]]
        gathered.append(slab.reshape(*slab.shape[:along], *a.shape[along:]))
        at += column.shape[along]
    return tuple(gathered)


def rounded(matrix):
    return lax.optimization_barrier(matrix.astype(jnp.bfloat16)).astype(jnp.float32)


def contract(left, right):
    return lax.dot_general(
        left, right, (((1,), (1,)), ((), ())), preferred_element_type=jnp.float32
    )


def divide_among_attention_units(matrix, head_width):
    return jnp.transpose(matrix.reshape(matrix.shape[0], -1, head_width), (1, 0, 2))


def blockwise(query_rows, key_rows, value_rows, log_decay, initial_state):
    head_count, length, key_width = query_rows.shape
    block_count = length // BLOCK

    def to_blocks(tensor):
        return jnp.moveaxis(tensor.reshape(head_count, block_count, BLOCK, tensor.shape[-1]), 1, 0)

    lower_mask = jnp.tril(jnp.ones((BLOCK, BLOCK), jnp.float32))

    def advance(current_state, inputs):
        query_block, key_block_rows, value_block_rows, decay_block = inputs
        cumulative_logs = jnp.cumsum(decay_block, axis=1)
        block_finish = cumulative_logs[:, -1:, :]
        decayed_query_rows = query_block * jnp.exp(cumulative_logs)
        scores = (
            jnp.einsum(
                "hck,hsk->hcs",
                decayed_query_rows,
                key_block_rows * jnp.exp(-cumulative_logs),
                precision=highest_precision,
            )
            * lower_mask
        )
        output_rows = jnp.einsum(
            "hcs,hsv->hcv", scores, value_block_rows, precision=highest_precision
        )
        output_rows = output_rows + jnp.einsum(
            "sei,siw->sew", decayed_query_rows, current_state, precision=highest_precision
        )
        current_state = jnp.exp(block_finish[:, 0, :])[:, :, None] * current_state + jnp.einsum(
            "zoa,zol->zal",
            key_block_rows * jnp.exp(block_finish - cumulative_logs),
            value_block_rows,
            precision=highest_precision,
        )
        return (current_state, output_rows)

    final_state, outputs = lax.scan(
        advance,
        initial_state,
        (to_blocks(query_rows), to_blocks(key_rows), to_blocks(value_rows), to_blocks(log_decay)),
    )
    return (jnp.moveaxis(outputs, 0, 1).reshape(head_count, length, -1), final_state)


def entering(log_totals, state_rows, place):
    cumulative_logs = jnp.cumsum(log_totals, axis=0)
    before = lax.dynamic_index_in_dim(cumulative_logs, place - 1, 0, keepdims=False)
    position = jnp.arange(log_totals.shape[0])
    exponent_value = jnp.where(
        (position < place)[:, None, None], before[None] - cumulative_logs, -jnp.inf
    )
    return jnp.einsum(
        "aqb,aqbm->qbm", jnp.exp(exponent_value), state_rows, precision=highest_precision
    )


def per_device(
    latent,
    context,
    cond,
    ctx_cond,
    w_shift,
    w_scale,
    w_gate,
    norm_gain,
    w_query,
    w_key,
    w_value,
    w_decay_fwd,
    w_decay_bwd,
    forgetting_shift_vector,
    decay_log,
    head_gain,
    w_out,
):
    tok_rows, channels = latent.shape
    heads_here = forgetting_shift_vector.shape[0] // ADDRESS_WIDTH
    key_columns = heads_here * ADDRESS_WIDTH
    value_columns = heads_here * VALUE_DIM
    activations = jnp.stack([jax.nn.silu(cond), jax.nn.silu(ctx_cond)]).astype(jnp.bfloat16)
    partials = jnp.stack(
        [
            jnp.dot(activations, weight, preferred_element_type=jnp.float32)
            for weight in (w_shift, w_scale, w_gate)
        ],
        axis=1,
    )
    wide_lat = latent.astype(jnp.float32)
    wide_ctx = context.astype(jnp.float32)
    squares_lat = jnp.sum(wide_lat * wide_lat, axis=1)
    squares_ctx = jnp.sum(wide_ctx * wide_ctx, axis=1)
    modulation = taken_together(partials, "sp")
    total_lat, total_ctx = together((squares_lat, squares_ctx), "tp")
    shift_full = modulation[:, 0].astype(jnp.bfloat16)
    inverse_lat = lax.rsqrt(total_lat / WIDTH + epsilon)[:, None]
    inverse_ctx = lax.rsqrt(total_ctx / WIDTH + epsilon)[:, None]
    scaled_lat = (wide_lat * (norm_gain * (1.0 + modulation[0, 1]))[None, :]).astype(jnp.bfloat16)
    scaled_ctx = (wide_ctx * (norm_gain * (1.0 + modulation[1, 1]))[None, :]).astype(jnp.bfloat16)
    w_local = jnp.concatenate([w_query, w_key, w_value, w_decay_fwd, w_decay_bwd], axis=0)
    members = (scaled_lat, scaled_ctx, shift_full)
    pieces = gather_turned((members[0], members[1], members[2]), "tp", (1, 1, 1))
    w_rows = w_local
    folded = tuple((contract(member, w_rows) for member in pieces))
    main_lat, main_ctx, shift_part = folded
    proj_lat = inverse_lat * main_lat + shift_part[0][None, :]
    proj_ctx = inverse_ctx * main_ctx + shift_part[1][None, :]
    value_end = 2 * key_columns + value_columns
    query_rows = divide_among_attention_units(
        rounded(proj_lat[:, :key_columns]), ADDRESS_WIDTH
    ) * ADDRESS_WIDTH ** (-0.5)
    key_lat = divide_among_attention_units(
        rounded(proj_lat[:, key_columns : 2 * key_columns]), ADDRESS_WIDTH
    )
    value_lat = divide_among_attention_units(
        rounded(proj_lat[:, 2 * key_columns : value_end]), VALUE_DIM
    )
    context_key_rows = divide_among_attention_units(
        rounded(proj_ctx[:, key_columns : 2 * key_columns]), ADDRESS_WIDTH
    )
    context_value_rows = divide_among_attention_units(
        rounded(proj_ctx[:, 2 * key_columns : value_end]), VALUE_DIM
    )
    summand_list = jnp.transpose(decay_log)[:, :, None]

    def log_decays(projected, offset):
        unprocessed_entries = (
            projected[:, offset : offset + key_columns] + forgetting_shift_vector[None, :]
        )
        return divide_among_attention_units(
            jax.nn.log_sigmoid(unprocessed_entries) / smoothing_scale_factor, ADDRESS_WIDTH
        )

    onward_logarithms = log_decays(proj_lat, value_end) + summand_list
    reverse_logarithms = log_decays(proj_lat, value_end + key_columns) + summand_list
    conditioning_onward_logarithms = log_decays(proj_ctx, value_end)
    conditioning_reverse_logarithms = log_decays(proj_ctx, value_end + key_columns)
    zero_state = jnp.zeros((heads_here, ADDRESS_WIDTH, VALUE_DIM), jnp.float32)
    fwd_out, fwd_state = blockwise(query_rows, key_lat, value_lat, onward_logarithms, zero_state)
    flip_queries = jnp.flip(query_rows, 1)
    flip_logb = jnp.flip(reverse_logarithms, 1)
    bwd_out, bwd_state = blockwise(
        flip_queries, jnp.flip(key_lat, 1), jnp.flip(value_lat, 1), flip_logb, zero_state
    )
    fwd_total = jnp.sum(onward_logarithms, axis=1)
    bwd_total = jnp.sum(reverse_logarithms, axis=1)
    cumulative_forward = jnp.cumsum(conditioning_onward_logarithms, axis=1)
    ctx_fwd_state = jnp.einsum(
        "xcq,xcs->xqs",
        context_key_rows * jnp.exp(cumulative_forward[:, -1:, :] - cumulative_forward),
        context_value_rows,
        precision=highest_precision,
    )
    cumulative_backward = jnp.cumsum(conditioning_reverse_logarithms, axis=1)
    ctx_bwd_state = jnp.einsum(
        "xcq,xcs->xqs",
        context_key_rows * jnp.exp(cumulative_backward - conditioning_reverse_logarithms),
        context_value_rows,
        precision=highest_precision,
    )
    ctx_fwd_total = cumulative_forward[:, -1, :]
    ctx_bwd_total = cumulative_backward[:, -1, :]
    log_stack = jnp.stack([fwd_total, bwd_total, ctx_fwd_total, ctx_bwd_total])[None]
    state_stack = jnp.stack([fwd_state, bwd_state, ctx_fwd_state, ctx_bwd_state])[None]
    all_logs, all_states = tuple(
        (
            part.astype(jnp.float32)
            for part in in_one_piece(
                (log_stack.astype(jnp.bfloat16), state_stack.astype(jnp.bfloat16)), "sp", 0, 4
            )
        )
    )
    block_total = all_logs.shape[0]
    block_place = lax.axis_index("sp")
    fwd_logs = jnp.concatenate([all_logs[:, 2], all_logs[:, 0]], axis=0)
    fwd_states = jnp.concatenate([all_states[:, 2], all_states[:, 0]], axis=0)
    bwd_logs = jnp.concatenate([jnp.flip(all_logs[:, 3], 0), jnp.flip(all_logs[:, 1], 0)], axis=0)
    bwd_states = jnp.concatenate(
        [jnp.flip(all_states[:, 3], 0), jnp.flip(all_states[:, 1], 0)], axis=0
    )
    entering_forward = entering(fwd_logs, fwd_states, block_total + block_place)
    enter_bwd = entering(bwd_logs, bwd_states, 2 * block_total - 1 - block_place)
    fwd_mixed = fwd_out + jnp.einsum(
        "dwz,dzn->dwn",
        query_rows * jnp.exp(jnp.cumsum(onward_logarithms, axis=1)),
        entering_forward,
        precision=highest_precision,
    )
    bwd_mixed = bwd_out + jnp.einsum(
        "dwz,dzn->dwn",
        flip_queries * jnp.exp(jnp.cumsum(flip_logb, axis=1)),
        enter_bwd,
        precision=highest_precision,
    )
    mixed = fwd_mixed + jnp.flip(bwd_mixed, 1)
    normed = mixed * lax.rsqrt(jnp.mean(mixed * mixed, axis=2, keepdims=True) + epsilon)
    normed = normed * head_gain.reshape(heads_here, 1, VALUE_DIM)
    head_rows = (
        jnp.transpose(normed, (1, 0, 2)).reshape(tok_rows, value_columns).astype(jnp.bfloat16)
    )
    w_rows = w_out
    projected = contract(lax.all_gather(head_rows, "tp", axis=1, tiled=True), w_rows)
    return (modulation[0, 2][None, :] * projected).astype(jnp.bfloat16)


def solution(mesh):
    return jax.shard_map(
        per_device,
        mesh=mesh,
        in_specs=(
            P("sp", "tp"),
            P("sp", "tp"),
            P("sp"),
            P("sp"),
            P("sp", "tp"),
            P("sp", "tp"),
            P("sp", "tp"),
            P("tp"),
            P("tp", None),
            P("tp", None),
            P("tp", None),
            P("tp", None),
            P("tp", None),
            P("tp"),
            P("sp", "tp"),
            P("tp"),
            P("tp", None),
        ),
        out_specs=P("sp", "tp"),
        check_vma=False,
    )
```

profile of v0, /device:TPU:1, one launch (start us, length us, event | category | flops | bytes accessed | tf_op | source)
XLA Modules:
  0.0 326.3 jit_solution(405188996469516319)
XLA Ops:
  6.5 0.8 fusion.134
  7.3 0.7 fusion.135
  8.0 0.9 convolution_bitcast_fusion.2
  8.9 0.9 convolution_bitcast_fusion.3
  9.8 0.9 convolution_bitcast_fusion.4
  10.9 30.6 %all_to_all.11 = f32[16,1,384]{2,1,0:T(1,128)S(1)} all-to-all(f32[16,1,384]{2,1,0:T(1,128)S(1)} %reshape.567), channel_id=1, replica_groups=mesh['sp'=16,'tp'=64] {'sp'}, dimensions={0} | all-to-all | bytes 49152 | tf_op jit(solution)/shard_map/all_to_all | solution.py:19
  41.5 0.5 broadcast.221
  42.0 0.7 reduce.15
  42.9 0.7 fusion.140
  43.5 0.8 fusion.117
  44.5 1.0 fusion.92
  45.5 0.7 pad_maximum_fusion
  46.3 0.7 reduce.8
  47.0 0.5 iota_compare_fusion.3
  47.5 0.5 iota_compare_fusion.2
  48.0 1.0 constant_dynamic-update-slice_fusion.4
  49.2 0.8 broadcast_in_dim.42
  50.0 12.2 %all-to-all-start.1 = ((f32[64,1,800]{2,1,0:T(1,128)}), f32[64,1,800]{2,1,0:T(1,128)S(1)}, u32[]{:S(2)}, u32[]{:S(2)}) async-start(f32[64,1,800]{2,1,0:T(1,128)} %broadcast_in_dim.42), calls=%async_computation.1 | async-start | bytes 458752 | tf_op jit(solution)/shard_map/all_to_all | solution.py:19
  62.3 13.5 %all-to-all-done.1 = f32[64,1,800]{2,1,0:T(1,128)S(1)} async-done(((f32[64,1,800]{2,1,0:T(1,128)}), f32[64,1,800]{2,1,0:T(1,128)S(1)}, u32[]{:S(2)}, u32[]{:S(2)}) %all-to-all-start.1) | async-done | bytes 204832 | tf_op jit(solution)/shard_map/all_to_all | solution.py:19
  76.0 61.3 %all-gather.3.cloned.1.call-done = bf16[4096,802]{1,0:T(8,128)(2,1)} async-done(((bf16[64,802]{1,0:T(8,128)(2,1)}), bf16[4096,802]{1,0:T(8,128)(2,1)}) %all-gather.3.cloned.1.call-update) | async-done | bytes 6570000 | tf_op jit(solution)/shard_map/all_gather | solution.py:41
  137.3 2.4 fusion.86
  139.6 5.0 %fusion.150 = (bf16[768,192]{0,1:T(8,128)(2,1)S(1)}, f32[768,192]{0,1:T(8,128)}) fusion(f32[192]{0:T(256)S(1)} %bitcast.440, bf16[192,4096]{1,0:T(8,128)(2,1)S(1)} %constant_dynamic-update-slice_fusion, bf16[4096,802]{1,0:T(8,128)(2,1)} %all-gather.3.cloned.1.call-done, f32[768]{0:T(1024)S(1)} %add_rsqrt_fusion.1), kind=kOutput, calls=%fused_computation.230 | convolution fusion | flops 1208401920 | bytes 8752896 | tf_op jit(solution)/shard_map/dot_general | solution.py:65
  144.6 0.7 broadcast_multiply_fusion.1
  145.3 0.4 reverse.19
  145.9 2.1 reverse.17
  148.2 2.2 reverse.18
  150.4 1.8 fusion.151
  152.4 0.5 slice_bitcast_fusion.11
  153.0 1.3 fusion.144
  154.3 0.4 reverse.16
  154.9 0.6 copy_bitcast_fusion
  156.1 11.4 %while.26 = (s32[]{:T(128)}, f32[1,32,64]{2,1,0:T(8,128)S(1)}, f32[12,1,64,64]{3,2,1,0:T(8,128)S(1)}, f32[12,1,64,32]{3,2,1,0:T(8,128)S(1)}, f32[12,1,64,32]{3,2...) while((s32[]{:T(128)}, f32[1,32,64]{2,1,0:T(8,128)S(1)}, ...), condition=%wide.region_6.7_spmd.clone, body=%wide.region_4.6_spmd.clone.sunk | while | flops 8030211 | bytes 537212 | solution.py:111
  167.7 1.1 copy.158
  169.1 11.4 %while.27 = (s32[]{:T(128)}, f32[1,32,64]{2,1,0:T(8,128)S(1)}, f32[12,1,64,64]{3,2,1,0:T(8,128)S(1)}, f32[12,1,64,32]{3,2,1,0:T(8,128)S(1)}, f32[12,1,64,32]{3,2...) while((s32[]{:T(128)}, f32[1,32,64]{2,1,0:T(8,128)S(1)}, ...), condition=%wide.region_15.16_spmd.clone, body=%wide.region_13.15_spmd.clone.sunk | while | flops 8030211 | bytes 537212 | solution.py:111
  180.5 0.3 fusion.84
  181.2 27.4 %all_gather.10 = bf16[16,4,1,32,65]{4,3,2,1,0:T(8,128)(2,1)S(1)} all-gather(bf16[1,4,1,32,65]{4,3,2,1,0:T(8,128)(2,1)S(1)} %maximum_bitcast_fusion.3), channel_id=1, replica_groups=mesh['sp'=16,'tp'=64] {'sp'}, dimensions={0}, use_global_device_ids=true | all-gather | bytes 282880 | tf_op jit(solution)/shard_map/all_gather | solution.py:52
  208.8 0.5 copy.166
  210.0 1.7 reduce-window.16
  212.3 0.8 fusion.88
  213.1 0.4 convolution_add_fusion.2
  213.4 0.5 reverse.20
  214.1 1.7 reduce-window.14
  216.3 0.8 fusion.90
  217.1 0.4 multiply_reduce_fusion
  217.6 0.7 multiply_convert_fusion
  218.3 0.7 slice_bitcast_fusion.10
  219.0 95.9 %all-gather.5.cloned.1.call-done = bf16[768,4096]{0,1:T(8,128)(2,1)} async-done(((bf16[768,64]{0,1:T(8,128)(2,1)}), bf16[768,4096]{0,1:T(8,128)(2,1)}) %all-gather.5.cloned.1.call-update) | async-done | bytes 6291472 | tf_op jit(solution)/shard_map/all_gather | solution.py:275
  314.9 4.6 %fusion.81 = bf16[768,64]{0,1:T(8,128)(2,1)} fusion(bf16[64,4096]{1,0:T(8,128)(2,1)S(1)} %copy-done, bf16[768,4096]{0,1:T(8,128)(2,1)} %all-gather.5.cloned.1.call-done, f32[64]{0:T(128)S(1)} %slice_bitcast_fusion.10), kind=kOutput, calls=%fused_computation.88 | convolution fusion | flops 402751488 | bytes 6914304 | tf_op jit(solution)/shard_map/dot_general | solution.py:65
  (314 shorter events, 25.9 us)
Async XLA Ops:
  6.5 308.3 %copy-start = (bf16[64,4096]{1,0:T(8,128)(2,1)S(1)}, bf16[64,4096]{1,0:T(8,128)(2,1)}, u32[]{:S(2)}) copy-start(bf16[64,4096]{1,0:T(8,128)(2,1)} %param.37) | copy-start | bytes 1572868
  6.5 42.5 %copy-start.5 = (bf16[32,4096]{1,0:T(8,128)(2,1)S(1)}, bf16[32,4096]{1,0:T(8,128)(2,1)}, u32[]{:S(2)}) copy-start(bf16[32,4096]{1,0:T(8,128)(2,1)} %param.30) | copy-start | bytes 786436
  6.5 42.5 %copy-start.2 = (bf16[64,4096]{1,0:T(8,128)(2,1)S(1)}, bf16[64,4096]{1,0:T(8,128)(2,1)}, u32[]{:S(2)}) copy-start(bf16[64,4096]{1,0:T(8,128)(2,1)} %param.31) | copy-start | bytes 1572868
  6.5 130.7 %all-gather.3.cloned.1.call-start = ((), (), s32[]{:S(2)}) async-start(), calls=%async_computation.2 | async-start | bytes 7454720 | tf_op jit(solution)/shard_map/all_gather | solution.py:41
  10.7 38.4 %copy-start.6 = (bf16[32,4096]{1,0:T(8,128)(2,1)S(1)}, bf16[32,4096]{1,0:T(8,128)(2,1)}, u32[]{:S(2)}) copy-start(bf16[32,4096]{1,0:T(8,128)(2,1)} %param.32) | copy-start | bytes 786436
  42.8 4.7 %copy-start.10 = (f32[2,3,64]{2,0,1:T(2,128)}, f32[2,3,64]{2,0,1:T(2,128)S(1)}, u32[]{:S(2)}) copy-start(f32[2,3,64]{2,0,1:T(2,128)S(1)} %bitcast_reduce_fusion) | copy-start | bytes 4612
  48.0 14.2 %copy-start.7 = (bf16[32,4096]{1,0:T(8,128)(2,1)S(1)}, bf16[32,4096]{1,0:T(8,128)(2,1)}, u32[]{:S(2)}) copy-start(bf16[32,4096]{1,0:T(8,128)(2,1)} %param.33) | copy-start | bytes 786436
  50.0 25.8 %all-to-all-start.1 = ((f32[64,1,800]{2,1,0:T(1,128)}), f32[64,1,800]{2,1,0:T(1,128)S(1)}, u32[]{:S(2)}, u32[]{:S(2)}) async-start(f32[64,1,800]{2,1,0:T(1,128)} %broadcast_in_dim.42), calls=%async_computation.1 | async-start | bytes 458752 | tf_op jit(solution)/shard_map/all_to_all | solution.py:19
  62.2 252.6 %all-gather.5.cloned.1.call-start = ((), (), s32[]{:S(2)}) async-start(), calls=%async_computation.3 | async-start | bytes 6389760 | tf_op jit(solution)/shard_map/all_gather | solution.py:275
  148.2 4.0 %copy-start.11 = (f32[32]{0:T(128)S(1)}, f32[32]{0:T(128)}, u32[]{:S(2)}) copy-start(f32[32]{0:T(128)} %param.34) | copy-start | bytes 388
  152.2 0.9 copy-start.8
  152.2 3.7 %copy-start.4 = (f32[768,32]{0,1:T(8,128)S(1)}, f32[768,32]{0,1:T(8,128)}, u32[]{:S(2)}) copy-start(f32[768,32]{0,1:T(8,128)} %broadcast_multiply_fusion.1) | copy-start | bytes 294916
  156.1 12.7 %copy-start.1 = (f32[768,64]{0,1:T(8,128)S(1)}, f32[768,64]{0,1:T(8,128)}, u32[]{:S(2)}) copy-start(f32[768,64]{0,1:T(8,128)} %reverse.18) | copy-start | bytes 589828
  169.0 11.5 %copy-start.9 = (f32[32,192]{1,0:T(8,128)S(1)}, f32[32,192]{1,0:T(8,128)}, u32[]{:S(2)}) copy-start(f32[32,192]{1,0:T(8,128)} %copy-done.8) | copy-start | bytes 73732
  169.0 11.5 %copy-start.12 = (f32[32]{0:T(128)S(1)}, f32[32]{0:T(128)}, u32[]{:S(2)}) copy-start(f32[32]{0:T(128)} %param.34) | copy-start | bytes 388
  169.0 11.8 %copy-start.16 = (f32[32]{0:T(128)S(1)}, f32[32]{0:T(128)}, u32[]{:S(2)}) copy-start(f32[32]{0:T(128)} %slice_bitcast_fusion.11) | copy-start | bytes 388
  208.7 0.7 copy-start.15
  208.7 1.0 copy-start.14
  208.8 1.2 copy-start.3
  214.1 3.5 %copy-start.13 = (f32[64]{0:T(128)S(1)}, f32[64]{0:T(128)}, u32[]{:S(2)}) copy-start(f32[64]{0:T(128)} %param.36) | copy-start | bytes 772
Sparse Core Ops, SparseCore 0:
  46.4 90.7 all-gather.2
  218.4 96.3 all-gather.4
where the time goes:
time: 327 us; the launch traced here: 326 us
  waiting for transfers between devices  171 us (52%)
  blocking collectives  58 us (18%)
  matrix products  37.6 us (11%)
  other arithmetic  16.6 us (5%)
  local copies, waits for them, and re-layouts  15.3 us (5%)
  between operations  14.1 us (4%)
  starting transfers between devices  12.3 us (4%)
    all_gather x1, waiting for transfers between devices, per_device(): lax.all_gather(head_rows, 'tp', axis=1, tiled=True)  95.9 us
    all_gather x1, waiting for transfers between devices, gather_turned(): out, at, gathered = (lax.all_gather(both, axis, axis=0, tiled=True), 0, [])  61.3 us
    all_to_all x1, blocking collectives, from_everyone(): lax.all_to_all(jnp.broadcast_to(shard[None], (count, *shard.shape)), axis...  30.6 us
    all_gather x1, blocking collectives, in_one_piece(): lax.all_gather(both, axis, axis=dim, tiled=True)  27.4 us
    dot_general x4, matrix products, contract(): lax.dot_general(left, right, (((1,), (1,)), ((), ())), preferred_element_...  13.7 us
    all_to_all x1, waiting for transfers between devices, from_everyone(): lax.all_to_all(jnp.broadcast_to(shard[None], (count, *shard.shape)), axis...  13.5 us
    all_to_all x1, starting transfers between devices, from_everyone(): lax.all_to_all(jnp.broadcast_to(shard[None], (count, *shard.shape)), axis...  12.2 us
    another operation x19, local copies, waits for them, and re-layouts  7 us
  transfers between devices with their start and end apart: 3, of which 3 were waited for; matrix products, arithmetic and copies ran while one was open for 1% of the time, Pallas kernels for 0%

commit v1 on v0

v1 whole, which is shorter than its diff:
```python
import functools
import heapq
from types import SimpleNamespace

import jax
import jax.numpy as jnp
from jax import lax
from jax.experimental import pallas as pl
from jax.experimental.pallas import tpu as pltpu
from jax.sharding import PartitionSpec as P

f32 = jnp.float32
bf16 = jnp.bfloat16
EPS = 1e-06
STREAMS = (("y", 48, 80), ("x", 0, 48))
FEATS = 128


def halves(n, swap):
    small = (n // 2) // 16 * 16
    return (n - small, small) if swap else (small, n - small)


def gather_plan(X, Y, streams, rate, latency=2.0):
    sizes = {"x": X, "y": Y}
    messages = {}

    def ring(part, axis, base, r0, rows, needs):
        n = sizes[axis]
        swap = (sum(base) % 2) == 1
        for sign in (1, -1):
            for hop in range(1, n // 2 + 1):
                a, b = r0, rows
                if 2 * hop == n:
                    first, second = halves(rows, swap)
                    a, b = (r0, first) if sign == 1 else (r0 + first, second)
                offset = list(base)
                offset[0 if axis == "x" else 1] = sign * hop
                before = [(part, axis, base, sign, hop - 1)] if hop > 1 else list(needs)
                messages[(part, axis, base, sign, hop)] = dict(
                    axis=axis, sign=sign, hop=hop, offset=tuple(offset), a=a, n=b, before=before,
                    left=n // 2 - hop + (10 if part[0] == 1 else 0),
                )

    def origins(axis):
        n = sizes[axis]
        return [h for h in range(-(n // 2) + 1, n // 2 + 1)]

    def arrivals(part, axis, base, value):
        n = sizes[axis]
        if value == 0:
            return []
        if 2 * value == n:
            return [(part, axis, base, s, n // 2) for s in (1, -1)]
        return [(part, axis, base, 1 if value > 0 else -1, abs(value))]

    zero = (0, 0)
    for i, (axis, r0, rows) in enumerate(streams):
        ring((1, i), axis, zero, r0, rows, [])
        for v in origins(axis):
            base = (v, 0) if axis == "x" else (0, v)
            ring((2, i), "y" if axis == "x" else "x", base, r0, rows, arrivals((1, i), axis, zero, v))

    return simulate(messages, 768, rate, latency)


def simulate(messages, row_bytes, rate, latency):
    keys = list(messages)
    index = {k: i for i, k in enumerate(keys)}
    free = {(a, s): 0.0 for a in ("x", "y", "all") for s in (1, -1)}
    got, order, started, heap = set(), [], set(), []

    def launch(now):
        ready = [k for k in keys if k not in started and all(b in got for b in messages[k]["before"])]
        ready.sort(key=lambda k: -messages[k]["left"])
        for k in ready:
            m = messages[k]
            link = (m["axis"], m["sign"])
            begin = max(now, free[link])
            hops = m.get("step", 1)
            free[link] = begin + hops * m["n"] * row_bytes / rate
            heapq.heappush(heap, (free[link] + latency + 0.8 * (hops - 1), index[k]))
            started.add(k)
        return [index[k] for k in ready]

    first = launch(0.0)
    steps = []
    while heap:
        now, i = heapq.heappop(heap)
        got.add(keys[i])
        steps.append((i, launch(now), now))
    table = [messages[k] for k in keys]
    return table, first, steps


def share_plan(X, Y, rows, rate, latency=2.0):
    messages = {}
    half = Y // 2
    for v in range(-(X // 2) + 1, X // 2 + 1):
        if v:
            messages[("all", v)] = dict(axis="all", sign=1 if v > 0 else -1, offset=(v, 0), a=0, n=rows, before=[], left=20)
        for sign in (1, -1):
            for hop in range(1, half + 1):
                a, b = 0, rows
                if 2 * hop == Y:
                    first, second = halves(rows, v % 2 == 1)
                    a, b = (0, first) if sign == 1 else (first, second)
                step = 2 if hop % 2 == 0 else 1
                before = [(v, sign, hop - step)] if hop > 2 else [("all", v)] if v else []
                messages[(v, sign, hop)] = dict(
                    axis="y", sign=sign, offset=(v, sign * hop), a=a, n=b, before=before, step=step,
                    left=10 * (half - hop >= 2 and step == 2) + step,
                )
    return simulate(messages, 256, rate, latency)


def rows_done(plan, X, Y):
    table, _, steps = plan
    left = {}
    for m in table:
        oy = m["offset"][1] % Y
        left[oy] = left.get(oy, 0) + 1
    out = []
    for i, _, _ in steps:
        oy = table[i]["offset"][1] % Y
        left[oy] -= 1
        out.append([oy] if left[oy] == 0 else [])
    return out


def split3(v):
    hi = v.astype(bf16)
    r = v - hi.astype(f32)
    mid = r.astype(bf16)
    return hi, mid, (r - mid.astype(f32)).astype(bf16)


def mm(a, b):
    return lax.dot_general(a, b, (((1,), (0,)), ((), ())), preferred_element_type=f32)


def nt(a, b):
    return lax.dot_general(a, b, (((1,), (1,)), ((), ())), preferred_element_type=f32)


def iota(shape, dim):
    return lax.broadcasted_iota(jnp.int32, shape, dim)


def kernel(dims, *refs):
    X, Y, Z, HALF, WIDTH = dims
    NC = X * Y
    TILES = HALF // 128
    NB = 2 * TILES
    GK = X * FEATS
    names = (
        "lat", "ctx", "cond", "cctx", "ws", "wc", "wg", "gain",
        "wq", "wk", "wv", "wf", "wb", "fsv", "dl", "hg",
        "wo", "out", "xg", "xs", "wall", "wog", "gcol", "acc",
        "acc2", "hrow", "hq", "res", "obuf", "ctxo", "ctxp", "ctxm", "ctxg",
        "vec", "fsb", "vecp", "wm", "cnd", "zblk", "zred", "mblk",
        "mrecv", "xyblk", "xyg", "dlv", "pst", "tst",
        "qst", "ost", "zs1", "zs1r", "zmsg", "zrcv", "zent", "ent",
        "cs1", "cs1r", "cmsg", "crcv", "crcv2", "cpk", "loc_sem", "dd_send", "dd_recv",
        "ag1_send", "ag1_recv", "ag2_send", "ag2_recv", "z_send", "z_recv", "xy_send", "xy_recv",
        "cx_send", "cx_recv", "zc_send", "zc_recv", "zl_send", "zl_recv", "wg_send", "wg_recv", "o_send", "o_recv",
    )
    r = SimpleNamespace(**dict(zip(names, refs, strict=True)))

    z = lax.axis_index("sp")
    tp = lax.axis_index("tp")
    c = lax.rem(tp, 2)
    chip = lax.div(tp, 2)
    x = lax.rem(chip, X)
    y = lax.div(chip, X)
    o = 1 - c

    def along_x(step):
        return at(z, lax.rem(x + step + X, X), y, c)

    scopes = []

    def mark(name):
        if scopes:
            scopes.pop().__exit__(None, None, None)
        if name:
            s = jax.named_scope(name)
            s.__enter__()
            scopes.append(s)

    mark("start")

    def at(zz, xx, yy, cc):
        return (zz, (yy * X + xx) * 2 + cc)

    partner = at(z, x, y, o)
    far = lambda d, n: min(d, n - d)
    zstep = sorted(range(1, Z), key=lambda j: -far(j, Z))
    zpeer = [at(lax.rem(z + j, Z), x, y, c) for j in zstep]
    offs = [(dx, dy) for dy in range(Y) for dx in range(X) if dx or dy]
    offs.sort(key=lambda d: -far(d[0], X) - far(d[1], Y))
    xypeer = [at(z, lax.rem(x + dx, X), lax.rem(y + dy, Y), c) for dx, dy in offs]

    def remote(src, dst, ssem, rsem, dev):
        return pltpu.make_async_remote_copy(
            src_ref=src, dst_ref=dst, send_sem=ssem, recv_sem=rsem,
            device_id=dev, device_id_type=pl.DeviceIdType.MESH,
        )

    def wait_sends(ref, ssem, rsem):
        remote(ref, ref, ssem, rsem, partner).wait_send()

    def wait_recvs(ref, ssem, rsem):
        remote(ref, ref, ssem, rsem, partner).wait_recv()

    half = pl.ds(pl.multiple_of(c * HALF, 128), HALF)
    other = pl.ds(pl.multiple_of(o * HALF, 128), HALF)
    wrows = (("wq", 0, 32), ("wk", 64, 32), ("wv", 128, 64), ("wf", 256, 32), ("wb", 320, 32))

    def mine(base, n):
        return pl.ds(pl.multiple_of(base + c * n, 16), n)

    local = []

    def bring(src, dst):
        cp = pltpu.make_async_copy(src, dst, r.loc_sem.at[len(local)])
        cp.start()
        local.append(cp)

    bring(r.cond, r.cnd.at[0])
    bring(r.cctx, r.cnd.at[1])
    bring(r.ws, r.wm.at[0])
    bring(r.wc, r.wm.at[1])
    bring(r.wg, r.wm.at[2])
    bring(r.gain, r.vec.at[0])
    bring(r.hg, r.vec.at[1])
    bring(r.fsv, r.fsb)
    n_first = len(local)
    bring(r.ctx.at[pl.ds(pl.multiple_of(c * 16, 16), 16)], r.ctxo)
    bring(r.lat.at[:, half], r.xg.at[chip, mine(0, 64)])
    n_second = len(local)
    bring(r.dl.at[:, half], r.dlv.at[0])
    for name, base, n in wrows:
        bring(getattr(r, name), r.wall.at[mine(base, n)])
    bring(r.wo, r.wog.at[x, mine(0, 64)])

    barrier = pltpu.get_barrier_semaphore()
    peers = [partner] + xypeer + zpeer
    for dev in peers:
        pl.semaphore_signal(barrier, inc=1, device_id=dev, device_id_type=pl.DeviceIdType.MESH)
    for cp in local[:n_first]:
        cp.wait()

    kw = r.cnd.shape[2]
    row8 = iota((8, kw), 0)
    cl = r.cnd[0]
    cc = r.cnd[1]
    al = (cl * jax.nn.sigmoid(cl)).astype(bf16).astype(f32)
    ac = (cc * jax.nn.sigmoid(cc)).astype(bf16).astype(f32)
    act = jnp.where(row8 == 1, jnp.broadcast_to(ac, (8, kw)), jnp.broadcast_to(al, (8, kw))).astype(bf16)
    d1 = nt(act, jnp.concatenate([r.wm[0], r.wm[1]], axis=0))
    d2 = nt(act, jnp.concatenate([r.wm[2], r.wm[2]], axis=0))
    r8 = iota((8, 128), 0)
    l8 = iota((8, 128), 1)
    part = jnp.where(r8 < 2, d1, d2)
    r.zblk[...] = part
    hg64 = r.vec[1]
    gn64 = r.vec[0]
    hgd = jnp.concatenate([hg64, hg64], axis=1)
    gnd = jnp.concatenate([gn64, gn64], axis=1)
    f1 = r.fsb[...]
    fsd = jnp.concatenate([f1, f1, f1, f1], axis=1)
    vown = jnp.where(r8 == 0, hgd, jnp.where(r8 == 1, fsd, gnd))
    r.mblk[pl.ds(16, 8)] = vown

    mark("barrier")
    pl.semaphore_wait(barrier, len(peers))

    mark("sends")
    for j, dev in enumerate(zpeer):
        cp = remote(r.zblk.at[pl.ds(0, 4)], r.zred.at[z, pl.ds(0, 4)], r.z_send, r.z_recv, dev)
        cp.start()
    dd = []

    def give(src, dst):
        k = len(dd)
        cp = remote(src, dst, r.dd_send.at[k], r.dd_recv.at[k], partner)
        cp.start()
        dd.append(cp)
        return cp

    d_lat = give(r.lat.at[:, other], r.xg.at[chip, mine(0, 64)])
    d_ctx = give(r.ctx.at[pl.ds(pl.multiple_of(o * 16, 16), 16)], r.ctxp)
    for cp in local[n_first:n_second]:
        cp.wait()

    plan = gather_plan(X, Y, STREAMS, 42.0e3, 2.8)
    table = plan[0]

    def gather(plan, buf, ssem, rsem, after):
        table, first, steps = plan
        copies = {}

        def slot_of(ox, oy):
            return lax.rem(y - oy + Y, Y) * X + lax.rem(x - ox + X, X)

        def go(i):
            m = table[i]
            ox, oy = m["offset"]
            if m["axis"] == "all":
                to = lax.rem(x + ox + X, X)
                src = r.hrow.at[pl.ds(pl.multiple_of(to * m["n"], 16), m["n"])]
                dst, dev = buf.at[chip], along_x(ox)
            else:
                if m["axis"] == "x":
                    dev = along_x(m["sign"])
                    slot = slot_of(ox - m["sign"], oy)
                else:
                    step = m["sign"] * m.get("step", 1)
                    dev = at(z, x, lax.rem(y + step + Y, Y), c)
                    slot = slot_of(ox, oy - step)
                src = dst = buf.at[slot, pl.ds(m["a"], m["n"])]
            copies[i] = remote(src, dst, ssem, rsem.at[i], dev)
            copies[i].start()

        for i in first:
            go(i)
        after(-1, 0.0)
        for s, (i, then, when) in enumerate(steps):
            m = table[i]
            ref = buf.at[slot_of(*m["offset"]), pl.ds(m["a"], m["n"])]
            wait_recvs(ref, ssem, rsem.at[i])
            for k in then:
                go(k)
            after(s, when)
        return copies

    lane128 = l8[:1]
    mylane = lane128 // 64 == c

    def join(own, recv, lanes):
        return jnp.where(lanes // 64 == c, own, recv)

    state = {}

    def send_ctx():
        d_ctx.wait_recv()
        own = r.ctxo[...].astype(f32)
        rec = r.ctxp[...].astype(f32)
        lo = jnp.where(c == 0, own, rec)
        hi = jnp.where(c == 0, rec, own)
        both = jnp.concatenate([lo, hi], axis=1).astype(bf16)
        r.ctxm[...] = both
        r.ctxg[chip] = both
        for j, dev in enumerate(xypeer):
            cp = remote(r.ctxm, r.ctxg.at[chip], r.cx_send, r.cx_recv, dev)
            cp.start()

    def send_weights():
        state["wd1"] = [give(getattr(r, name), r.wall.at[mine(base, n)]) for name, base, n in wrows]
        state["wd1"].append(give(r.dl.at[:, other], r.dlv.at[1]))
        state["wd1"].append(give(r.wo, r.wog.at[x, mine(0, 64)]))

    def z_sum():
        wait_recvs(r.zred.at[pl.ds(0, Z - 1), pl.ds(0, 4)], r.z_send, r.z_recv)
        r.zred[z] = part
        M = r.zred[0][0:4]
        for j in range(1, Z):
            M = M + r.zred[j][0:4]
        M = jnp.concatenate([M, M], axis=0)
        rM = pltpu.roll(M, 64, 1)
        r.mblk[pl.ds(0, 8)] = jnp.where(l8 < 64, M, rM)
        r.mblk[pl.ds(8, 8)] = jnp.where(l8 < 64, rM, M)
        state["mod"] = give(r.mblk, r.mrecv)

    def xy_send():
        state["mod"].wait_recv()
        lanes = iota((24, 128), 1)
        rws = iota((24, 128), 0)
        pick = jnp.where(rws == 17, (lanes // 32) % 2, lanes // 64)
        both = jnp.where(pick == c, r.mblk[...], r.mrecv[...])
        A = both[0:8]
        B = both[8:16]
        V = both[16:24]
        r.vecp[...] = jnp.where(r8 < 2, V, jnp.where(r8 == 2, A, 0.0))
        G = V[2:3] * (1.0 + B)
        blk = jnp.where(r8 < 2, A, jnp.where(r8 < 4, pltpu.roll(G, 2, 0), pltpu.roll(A, 2, 0)))
        r.xyblk[...] = blk
        r.xyg[chip] = blk
        for j, dev in enumerate(xypeer):
            cp = remote(r.xyblk, r.xyg.at[chip], r.xy_send, r.xy_recv, dev)
            cp.start()

    def w_part(slot, a, n):
        return r.wog.at[lax.rem(slot + X, X), pl.ds(pl.multiple_of(c * 64 + a, 16), n)]

    wg = []

    def w_ring(sign, slot, a, n):
        k = len(wg)
        ref = w_part(slot, a, n)
        cp = remote(ref, ref, r.wg_send.at[k], r.wg_recv.at[k], along_x(sign))
        cp.start()
        wg.append((cp, slot - sign, a, n))

    def w_landed(k):
        _, slot, a, n = wg[k]
        ref = w_part(slot, a, n)
        remote(ref, ref, r.wg_send.at[k], r.wg_recv.at[k], partner).wait_recv()
        return give(ref, ref)

    def w_first():
        if X == 2:
            w_ring(1, x, 0, 32)
            w_ring(-1, x, 32, 32)
        else:
            w_ring(1, x, 0, 64)
            w_ring(-1, x, 0, 64)

    def w_second():
        state["wd"] = [w_landed(0), w_landed(1)]
        if X == 4:
            w_ring(1, x - 1, 0, 32)
            w_ring(-1, x + 1, 32, 32)

    def w_third():
        if X == 4:
            state["wd"] += [w_landed(2), w_landed(3)]
        for cp in state["wd"]:
            cp.wait_recv()

    def cols_of(v):
        return jnp.transpose(jnp.concatenate([v, jnp.zeros((120, 128), f32)], axis=0))

    row128 = iota((128, 128), 0)
    ln128 = iota((128, 128), 1)
    same = (row128 // 64) == (ln128 // 64)
    tri = jnp.where(same & (row128 <= ln128), 1.0, 0.0).astype(bf16)
    blk_ones = jnp.where(same, 1.0, 0.0).astype(bf16)
    sums = jnp.concatenate([tri, blk_ones], axis=1)
    ind = jnp.where((r8 < 2) & (l8 // 64 == r8), 1.0, 0.0).astype(bf16)
    head_lane = (lane128 // 32) % 2
    mf = same & (row128 <= ln128)
    mb = same & (row128 >= ln128)

    def exponents(L):
        hi, mid, lo = split3(L)
        big = mm(jnp.concatenate([hi, mid, lo], axis=0), sums)
        big = big[0:128] + big[128:256] + big[256:384]
        C, T = big[:, 0:128], big[:, 128:256]
        E = jnp.where(row128 < 64, C, T - C + L)
        tot = nt(ind, hi) + nt(ind, mid) + nt(ind, lo)
        return E, T - E, tot

    def terms(k2, vT, D):
        ks = k2 * jnp.exp(D)
        stack = jnp.concatenate(
            [jnp.where(ln128 < 64, ks, 0.0).astype(bf16), jnp.where(ln128 < 64, 0.0, ks).astype(bf16)], axis=0
        )
        K = nt(vT, stack)
        first = jnp.where(head_lane == 0, K[0:64, 0:128], K[64:128, 0:128])
        second = jnp.where(head_lane == 0, K[0:64, 128:256], K[64:128, 128:256])
        return first, second

    def log_sigmoid(v):
        return jnp.minimum(v, 0.0) - jnp.log1p(jnp.exp(-jnp.abs(v)))

    lane64 = iota((64, 128), 1)
    lane32 = iota((32, 128), 1)
    lane16 = iota((16, 128), 1)

    def chip_state(stage, recv, own_ref):
        own = own_ref[pl.ds(pl.multiple_of(c * 32, 8), 32)]
        rec = recv[pl.ds(0, 32)]
        town = stage[pl.ds(32, 1)]
        trec = recv[pl.ds(32, 1)]
        s0 = jnp.where(c == 0, own, rec)
        s1 = jnp.where(c == 0, rec, own)
        t0 = jnp.where(c == 0, town, trec)
        t1 = jnp.where(c == 0, trec, town)
        both = jnp.where(lane32 < 64, jnp.exp(t1) * s0 + s1, jnp.exp(t0) * s1 + s0)
        return both, t0, t1, s0, s1

    def log_rows(T):
        hi = T.astype(bf16).astype(f32)
        return jnp.where(iota((16, 128), 0) == 0, hi, jnp.where(iota((16, 128), 0) == 1, T - hi, 0.0))

    def mod_in():
        wait_recvs(r.xyg.at[pl.ds(0, NC - 1)], r.xy_send, r.xy_recv)
        wait_recvs(r.ctxg.at[pl.ds(0, NC - 1)], r.cx_send, r.cx_recv)
        for cp in local[n_second:]:
            cp.wait()
        for cp in state["wd1"]:
            cp.wait_recv()

        for q in range(max(NC // 16, 1)):
            n = min(NC, 16)
            rows = r.xyg[pl.ds(q * n, n)].reshape(n * 8, 128)
            if n < 16:
                rows = jnp.concatenate([rows, jnp.zeros((128 - n * 8, 128), f32)], axis=0)
            t = jnp.transpose(rows)
            for b in range(n):
                r.gcol[q * n + b] = jnp.broadcast_to(t[:, b * 8 + 2 : b * 8 + 3], (128, 128))

    def ctx_work(sq):
        pcv = r.acc[:, pl.ds(HALF, 128)]
        sqt = jnp.transpose(jnp.concatenate([sq, jnp.zeros((112, 128), f32)], axis=0))
        ssum = jnp.sum(sqt, axis=0, keepdims=True)
        inv = lax.rsqrt(ssum / WIDTH + EPS)
        cp_ = inv * pcv + pcv[:, 17:18]
        valid = ln128 < 16
        k = jnp.where(valid[0:64], cp_[64:128], 0.0).astype(bf16).astype(f32)
        k2 = jnp.concatenate([k, k], axis=0)
        vT = jnp.where(valid, cp_[128:256], 0.0).astype(bf16)
        colv = cols_of(r.vecp[...])
        L = jnp.where(valid, log_sigmoid(cp_[256:384] + colv[:, 1:2]) / 16.0, 0.0)
        E, D, tot = exponents(L)
        first, _ = terms(k2, vT, D)
        r.cpk[...] = first
        r.cs1[pl.ds(0, 32)] = jnp.where(c == 0, first[32:64], first[0:32])
        r.cs1[pl.ds(32, 8)] = jnp.broadcast_to(tot[0:1], (8, 128))
        state["c1"] = give(r.cs1, r.cs1r)

    G = min(4, Z)
    za, zb = lax.div(z, G), lax.rem(z, G)

    def ctx_message(both, T):
        return jnp.concatenate([both, log_rows(T)[0:8]], axis=0).astype(bf16)

    def ctx_fold(ref, n):
        sf = sb = T = None
        for i in range(n):
            m = ref[i].astype(f32)
            t = m[32:33] + m[33:34]
            sf = m[0:32] if i == 0 else jnp.exp(t) * sf + m[0:32]
            T = t if i == 0 else T + t
            m = ref[n - 1 - i].astype(f32)
            sb = m[0:32] if i == 0 else jnp.exp(m[32:33] + m[33:34]) * sb + m[0:32]
        return jnp.where(lane32 < 64, sf, sb), T

    def ctx_send():
        state["c1"].wait_recv()
        both, t0, t1, _, _ = chip_state(r.cs1, r.cs1r, r.cpk)
        msg = ctx_message(both, t0 + t1)
        r.cmsg[0] = msg
        r.crcv[zb] = msg
        for j in range(1, G):
            dev = at(za * G + lax.rem(zb + j, G), x, y, c)
            cp = remote(r.cmsg.at[0], r.crcv.at[zb], r.zc_send.at[0], r.zc_recv.at[0], dev)
            cp.start()

    def ctx_second():
        wait_recvs(r.crcv.at[pl.ds(0, G - 1)], r.zc_send.at[0], r.zc_recv.at[0])
        both, T = ctx_fold(r.crcv, G)
        msg = ctx_message(both, T)
        r.cmsg[1] = msg
        r.crcv2[za] = msg
        for j in range(1, Z // G):
            dev = at(lax.rem(z + j * G, Z), x, y, c)
            cp = remote(r.cmsg.at[1], r.crcv2.at[za], r.zc_send.at[1], r.zc_recv.at[1], dev)
            cp.start()

    def ctx_done():
        if Z > G:
            wait_recvs(r.crcv2.at[pl.ds(0, Z // G - 1)], r.zc_send.at[1], r.zc_recv.at[1])
        r.cpk[pl.ds(0, 32)] = ctx_fold(r.crcv2, Z // G)[0]

    sums_of = {"lat": [jnp.zeros((8, 128), f32) for _ in range(TILES)], "ctx": jnp.zeros((16, 128), f32), "n": 0}

    def project(yy):
        for xx in range(X):
            b = yy * X + xx
            xr = pl.ds(xx * 128, 128)
            for t in range(TILES):
                v = r.xg[b, :, pl.ds(t * 128, 128)].astype(f32)
                s2 = v * v
                part_s = s2[0:8]
                for q in range(1, 16):
                    part_s = part_s + s2[q * 8 : q * 8 + 8]
                sums_of["lat"][t] = sums_of["lat"][t] + part_s
                r.xs[xr, pl.ds(t * 128, 128)] = (v * r.gcol[b]).astype(bf16)
            m = r.xyg[b]
            raw = r.ctxg[b].astype(f32)
            sums_of["ctx"] = sums_of["ctx"] + raw * raw
            rows = jnp.concatenate([raw * m[3:4], m, jnp.zeros((104, 128), f32)], axis=0)
            r.xs[xr, pl.ds(HALF, 128)] = jnp.transpose(rows).astype(bf16)
        step = mm(r.wall[:, pl.ds(pl.multiple_of(yy * GK, 128), GK)], r.xs[...])
        r.acc[...] = step if sums_of["n"] == 0 else r.acc[...] + step
        sums_of["n"] += 1

    actions = [(9.5, z_sum), (10.3, xy_send), (10.8, send_ctx), (12.0, send_weights)]
    pending = list(actions)
    rows1 = rows_done(plan, X, Y)
    last_go = max(i for i, st in enumerate(plan[2]) if st[1])
    waiting = []

    def after1(s, when):
        if s < 0:
            return
        while pending and pending[0][0] <= when:
            fn = pending.pop(0)[1]
            with jax.named_scope(fn.__name__):
                fn()
        waiting.extend(rows1[s])
        if s == last_go:
            while pending:
                pending.pop(0)[1]()
            with jax.named_scope("mod_in"):
                mod_in()
            w_first()
        if s >= last_go:
            while waiting:
                with jax.named_scope("project"):
                    project(lax.rem(y - waiting.pop(0) + Y, Y))

    mark("d_lat")
    d_lat.wait_recv()
    mark("ag1")
    copies1 = gather(plan, r.xg, r.ag1_send, r.ag1_recv, after1)
    ss = sums_of["lat"]

    mark("attend")
    colv = cols_of(r.vecp[...])
    shift_col = r.acc[:, pl.ds(HALF, 128)][:, 16:17]
    own_dl = r.dlv[0]
    rec_dl = r.dlv[1]
    dl0 = jnp.where(c == 0, own_dl, rec_dl)
    dl1 = jnp.where(c == 0, rec_dl, own_dl)
    for t in range(TILES):
        ts = pl.ds(t * 128, 128)
        inv = lax.rsqrt(jnp.sum(ss[t], axis=0, keepdims=True) / WIDTH + EPS)
        pr = inv * r.acc[:, ts] + shift_col
        q = pr[0:64].astype(bf16).astype(f32) * (32.0 ** -0.5)
        k = pr[64:128].astype(bf16).astype(f32)
        vT = pr[128:256].astype(bf16)
        q2 = jnp.concatenate([q, q], axis=0)
        k2 = jnp.concatenate([k, k], axis=0)
        dlt = jnp.where((row128 // 32) % 2 == 0, dl0[:, t * 128 : t * 128 + 128], dl1[:, t * 128 : t * 128 + 128])
        L = log_sigmoid(pr[256:384] + colv[:, 1:2]) / 16.0 + dlt
        E, D, tot = exponents(L)
        first, second = terms(k2, vT, D)
        r.pst[2 * t] = first
        r.pst[2 * t + 1] = second
        r.tst[t] = tot
        qf = q2 * jnp.exp(E)
        r.qst[t] = qf
        r.ost[t, 0] = k2 * jnp.exp(-E)
        r.ost[t, 1] = vT.astype(f32)

    T = [r.tst[i // 2][i % 2 : i % 2 + 1] for i in range(NB)]
    e = [jnp.exp(v) for v in T]
    sf = jnp.zeros((64, 128), f32)
    sb = jnp.zeros((64, 128), f32)
    for i in range(NB):
        sf = e[i] * sf + r.pst[i]
        sb = e[NB - 1 - i] * sb + r.pst[NB - 1 - i]
    seg = jnp.where(lane64 < 64, sf, sb)
    tseg = sum(T[1:], T[0])
    r.zent[...] = seg
    r.zs1[pl.ds(0, 32)] = jnp.where(c == 0, seg[32:64], seg[0:32])
    r.zs1[pl.ds(32, 8)] = jnp.broadcast_to(tseg, (8, 128))
    d_seg = give(r.zs1, r.zs1r)
    mark("ctx_work")
    ctx_work(sums_of["ctx"])
    mark("d_seg")
    ctx_send()
    d_seg.wait_recv()
    mark("combine")
    both, t0, t1, s0, s1 = chip_state(r.zs1, r.zs1r, r.zent)
    tc = t0 + t1
    rtc = pltpu.roll(jnp.broadcast_to(tc, (8, 128)), 64, 1)[0:1]
    ra = pltpu.roll(both[0:16], 64, 1)
    rb = pltpu.roll(both[16:32], 64, 1)
    r.zmsg[0] = jnp.concatenate(
        [jnp.where(lane16 < 64, both[0:16], rb), log_rows(jnp.where(lane128 < 64, tc, rtc))[0:8]], axis=0
    ).astype(bf16)
    r.zmsg[1] = jnp.concatenate(
        [jnp.where(lane16 < 64, ra, both[16:32]), log_rows(jnp.where(lane128 < 64, rtc, tc))[0:8]], axis=0
    ).astype(bf16)
    r.zrcv[z] = jnp.zeros((24, 128), bf16)
    for j, dev in enumerate(zpeer):
        behind = jnp.where(z + zstep[j] >= Z, 1, 0)
        cp = remote(r.zmsg.at[behind], r.zrcv.at[z], r.zl_send, r.zl_recv, dev)
        cp.start()

    mark("scores")
    for t in range(TILES):
        qf = r.qst[t]
        kdT = jnp.transpose(r.ost[t, 0]).astype(bf16)
        vT = r.ost[t, 1].astype(bf16)
        parts = [jnp.where(row128 // 32 == i, qf, 0.0).astype(bf16) for i in range(4)]
        AT = mm(kdT, jnp.concatenate(parts, axis=1))
        A0 = jnp.where(mf, AT[:, 0:128], 0.0) + jnp.where(mb, AT[:, 256:384], 0.0)
        A1 = jnp.where(mf, AT[:, 128:256], 0.0) + jnp.where(mb, AT[:, 384:512], 0.0)
        r.ost[t, 1] = jnp.concatenate(
            [mm(vT[0:64], A0.astype(bf16)), mm(vT[64:128], A1.astype(bf16))], axis=0
        )

    mark("ctx_second")
    ctx_second()
    mark("ctx_done")
    ctx_done()
    mark("zwait")
    wait_recvs(r.zrcv.at[pl.ds(0, Z - 1)], r.zl_send, r.zl_recv)
    mark("entering")
    ctxs = r.cpk[pl.ds(0, 32)]
    ca = pltpu.roll(ctxs[0:16], 64, 1)
    cb = pltpu.roll(ctxs[16:32], 64, 1)
    ef = jnp.where(lane16 < 64, ctxs[0:16], cb)
    eb = jnp.where(lane16 < 64, ca, ctxs[16:32])
    for s in range(Z):
        m = r.zrcv[s].astype(f32)
        ef = jnp.where(s < z, jnp.exp(m[16:17] + m[17:18]) * ef + m[0:16], ef)
        u = Z - 1 - s
        m = r.zrcv[u].astype(f32)
        eb = jnp.where(u > z, jnp.exp(m[16:17] + m[17:18]) * eb + m[0:16], eb)
    ech = jnp.concatenate(
        [
            jnp.where(lane16 < 64, ef, pltpu.roll(eb, 64, 1)),
            jnp.where(lane16 < 64, pltpu.roll(ef, 64, 1), eb),
        ],
        axis=0,
    )
    ent0 = jnp.where(lane32 < 64, ech, jnp.exp(t1) * ech + s1)
    ent1 = jnp.where(lane32 < 64, jnp.exp(t0) * ech + s0, ech)
    rows_c = pl.ds(pl.multiple_of(c * 32, 8), 32)
    d_seg.wait_send()
    r.zs1[pl.ds(0, 32)] = jnp.where(c == 0, ent1, ent0)
    r.ent[rows_c] = jnp.where(c == 0, ent0, ent1)
    mark("d_ent")
    d_ent = give(r.zs1.at[pl.ds(0, 32)], r.ent.at[rows_c])
    d_ent.wait_recv()

    mark("post")
    sf = r.ent[...]
    sb = sf
    fin, bin_ = [None] * NB, [None] * NB
    for i in range(NB):
        fin[i] = sf
        sf = e[i] * sf + r.pst[i]
        u = NB - 1 - i
        bin_[u] = sb
        sb = e[u] * sb + r.pst[u]
    hcol = colv[:, 0:1]
    for t in range(TILES):
        qf = r.qst[t]
        lhs = []
        for i in (2 * t, 2 * t + 1):
            s_in = jnp.where(lane64 < 64, fin[i], bin_[i])
            lhs.append(
                jnp.concatenate(
                    [jnp.where(head_lane == 0, s_in, 0.0), jnp.where(head_lane == 1, s_in, 0.0)], axis=0
                ).astype(bf16)
            )
        rhs = jnp.concatenate(
            [jnp.where(ln128 < 64, qf, 0.0).astype(bf16), jnp.where(ln128 < 64, 0.0, qf).astype(bf16)], axis=0
        )
        mixed = r.ost[t, 1] + mm(jnp.concatenate(lhs, axis=1), rhs)
        outs = []
        for h in range(2):
            mh = mixed[h * 64 : h * 64 + 64]
            outs.append(mh * lax.rsqrt(jnp.mean(mh * mh, axis=0, keepdims=True) + EPS))
        heads = jnp.concatenate(outs, axis=0) * hcol
        r.hrow[pl.ds(t * 128, 128)] = jnp.transpose(heads).astype(bf16)

    mark("ag2")
    TQ = HALF // X
    plan2 = share_plan(X, Y, TQ, 46.0e3, 2.8)
    r.hq[chip] = r.hrow[pl.ds(pl.multiple_of(x * TQ, 16), TQ)]
    done2 = rows_done(plan2, X, Y)
    ready2 = []

    def product(yy):
        heads = jnp.concatenate([r.hq[yy * X + xx] for xx in range(X)], axis=1)
        ks = pl.ds(pl.multiple_of(yy * GK, 128), GK)
        step = nt(r.wog[:, :, ks].reshape(X * 128, GK), heads)
        r.acc2[...] = step if not ready2 else r.acc2[...] + step
        ready2.append(yy)

    last_go2 = max([i for i, st in enumerate(plan2[2]) if st[1]], default=-1)
    waiting2 = []

    def after2(s, when):
        if s < 0:
            w_second()
            return
        waiting2.extend(done2[s])
        if s == len(plan2[2]) - 1:
            with jax.named_scope("w_third"):
                w_third()
            while waiting2:
                product(lax.rem(y - waiting2.pop(0) + Y, Y))

    copies2 = gather(plan2, r.hq, r.ag2_send, r.ag2_recv, after2)
    mark("final")
    gates = jnp.concatenate([r.xyg[y * X + xx][4:5] for xx in range(X)] + [jnp.zeros((8 - X, 128), f32)], axis=0)
    gates = cols_of(gates)
    for xx in range(X):
        piece = (r.acc2[pl.ds(xx * 128, 128)] * gates[:, xx : xx + 1]).astype(bf16)
        r.res[xx, 0] = piece[0:64]
        r.res[xx, 1] = piece[64:128]
    mine_at = 2 * x + c
    for dx, dc in [(dx, dc) for dx in (2, 1, 3, 0) if dx < X for dc in (0, 1) if dx or dc]:
        tx = lax.rem(x + dx, X)
        tc_ = lax.rem(c + dc, 2)
        cp = remote(
            r.res.at[tx, tc_], r.obuf.at[mine_at], r.o_send, r.o_recv, at(z, tx, y, tc_)
        )
        cp.start()
    r.obuf[mine_at] = r.res[x, c]
    wait_recvs(r.obuf.at[pl.ds(0, 2 * X - 1)], r.o_send, r.o_recv)
    r.out[...] = jnp.concatenate([r.obuf[2 * xx + cc_] for cc_ in (0, 1) for xx in range(X)], axis=1)
    mark("drain")
    for cp2 in dd:
        if cp2 is not d_seg:
            cp2.wait_send()
    wait_sends(r.zred.at[pl.ds(0, Z - 1), pl.ds(0, 4)], r.z_send, r.z_recv)
    wait_sends(r.ctxg.at[pl.ds(0, NC - 1)], r.cx_send, r.cx_recv)
    wait_sends(r.xyg.at[pl.ds(0, NC - 1)], r.xy_send, r.xy_recv)
    wait_sends(r.crcv.at[pl.ds(0, G - 1)], r.zc_send.at[0], r.zc_recv.at[0])
    if Z > G:
        wait_sends(r.crcv2.at[pl.ds(0, Z // G - 1)], r.zc_send.at[1], r.zc_recv.at[1])
    wait_sends(r.zrcv.at[pl.ds(0, Z - 1)], r.zl_send, r.zl_recv)
    wait_sends(r.obuf.at[pl.ds(0, 2 * X - 1)], r.o_send, r.o_recv)
    for cp2, _, _, _ in wg:
        cp2.wait_send()
    wait_sends(r.xg.at[pl.ds(0, NC - 1)], r.ag1_send, r.ag1_recv.at[0])
    wait_sends(r.hq.at[pl.ds(0, NC - 1)], r.ag2_send, r.ag2_recv.at[0])
    mark(None)


def per_device(
    latent, context, cond, ctx_cond, w_shift, w_scale, w_gate, norm_gain, w_query, w_key, w_value,
    w_decay_fwd, w_decay_bwd, forgetting_shift_vector, decay_log, head_gain, w_out,
):
    Z = lax.axis_size("sp")
    NC = lax.axis_size("tp") // 2
    X = 4 if NC >= 8 else 2
    Y = NC // X
    tok = latent.shape[0]
    HALF = tok // 2
    WIDTH = w_out.shape[1]
    dims = (X, Y, Z, HALF, WIDTH)
    TILES = HALF // 128
    M = len(gather_plan(X, Y, STREAMS, 46.0e3)[0])
    M2 = len(share_plan(X, Y, HALF // X, 46.0e3)[0])
    V = pltpu.VMEM
    D = pltpu.SemaphoreType.DMA
    GK = X * FEATS
    kw = cond.shape[0]
    scratch = [
        V((NC, 128, HALF), bf16),
        V((GK, HALF + 128), bf16),
        V((384, WIDTH), bf16),
        V((X, 128, WIDTH), bf16),
        V((NC, 128, 128), f32),
        V((384, HALF + 128), f32),
        V((X * 128, HALF // X), f32),
        V((HALF, 128), bf16),
        V((NC, HALF // X, 128), bf16),
        V((X, 2, 64, HALF // X), bf16),
        V((2 * X, 64, HALF // X), bf16),
        V((16, 64), bf16),
        V((16, 64), bf16),
        V((16, 128), bf16),
        V((NC, 16, 128), bf16),
        V((2, 1, 64), f32),
        V((1, 32), f32),
        V((8, 128), f32),
        V((3, 64, kw), bf16),
        V((2, 1, kw), f32),
        V((8, 128), f32),
        V((Z, 8, 128), f32),
        V((24, 128), f32),
        V((24, 128), f32),
        V((8, 128), f32),
        V((NC, 8, 128), f32),
        V((2, 1, HALF), f32),
        V((2 * TILES, 64, 128), f32),
        V((TILES, 8, 128), f32),
        V((TILES, 128, 128), f32),
        V((TILES, 2, 128, 128), f32),
        V((40, 128), f32),
        V((40, 128), f32),
        V((2, 24, 128), bf16),
        V((Z, 24, 128), bf16),
        V((64, 128), f32),
        V((64, 128), f32),
        V((40, 128), f32),
        V((40, 128), f32),
        V((2, 40, 128), bf16),
        V((4, 40, 128), bf16),
        V((4, 40, 128), bf16),
        V((64, 128), f32),
        D((17,)), D((17,)), D((17,)),
        D, D((M,)), D, D((M2,)),
        D, D, D, D, D, D,
        D((2,)), D((2,)), D, D,
        D((4,)), D((4,)), D, D,
    ]
    row = lambda v: v.reshape(1, -1)
    args = (
        latent.T, context, row(cond), row(ctx_cond), w_shift.T, w_scale.T, w_gate.T, row(norm_gain),
        w_query, w_key, w_value, w_decay_fwd, w_decay_bwd, row(forgetting_shift_vector), decay_log.T,
        row(head_gain), w_out,
    )
    out = pl.pallas_call(
        functools.partial(kernel, dims),
        out_shape=jax.ShapeDtypeStruct((64, tok), bf16),
        in_specs=[pl.BlockSpec(memory_space=pl.ANY)] * len(args),
        out_specs=pl.BlockSpec(memory_space=pltpu.VMEM),
        scratch_shapes=scratch,
        compiler_params=pltpu.CompilerParams(
            collective_id=0, has_side_effects=True, vmem_limit_bytes=56 * 1024 * 1024
        ),
        name="mixer",
    )(*args)
    return out.T


def solution(mesh):
    tp = P("tp")
    rows = P("tp", None)
    both = P("sp", "tp")
    return jax.shard_map(
        per_device,
        mesh=mesh,
        in_specs=(
            both, both, P("sp"), P("sp"), both, both, both, tp, rows, rows, rows, rows, rows, tp, both, tp, rows,
        ),
        out_specs=both,
        check_vma=False,
    )
```

time: 327 us -> 96.6 us (0.30)
  waiting for transfers between devices: 171 us -> 0 us
  Pallas kernels: 0 us -> 94.8 us
  blocking collectives: 58 us -> 0 us
  matrix products: 37.6 us -> 0 us
  other arithmetic: 16.6 us -> 0 us
  between operations: 14.1 us -> 0.01 us
  local copies, waits for them, and re-layouts: 15.3 us -> 1.54 us
  starting transfers between devices: 12.3 us -> 0 us
    all_gather x2 -> x0, waiting for transfers between devices: 157 us -> none  [the longest x1 95.9 us: per_device(): lax.all_gather(head_rows, 'tp', axis=1, tiled=True)]
    pallas_call x0 -> x1, Pallas kernels: none -> 94.8 us  [per_device(): pl.pallas_call(functools.partial(kernel, dims), out_shape=jax.ShapeDtypeS...]
    dot_general x109 -> x0, matrix products: 37.6 us -> none  [the longest x4 13.7 us: contract(): lax.dot_general(left, right, (((1,), (1,)), ((), ())), preferred_element_...]
    all_to_all x1 -> x0, blocking collectives: 30.6 us -> none  [from_everyone(): lax.all_to_all(jnp.broadcast_to(shard[None], (count, *shard.shape)), axis...]
    all_gather x1 -> x0, blocking collectives: 27.4 us -> none  [in_one_piece(): lax.all_gather(both, axis, axis=dim, tiled=True)]
    all_to_all x1 -> x0, waiting for transfers between devices: 13.5 us -> none  [from_everyone(): lax.all_to_all(jnp.broadcast_to(shard[None], (count, *shard.shape)), axis...]
    all_to_all x1 -> x0, starting transfers between devices: 12.2 us -> none  [from_everyone(): lax.all_to_all(jnp.broadcast_to(shard[None], (count, *shard.shape)), axis...]
    another operation x40 -> x0, other arithmetic: 7.67 us -> none
  transfers between devices with their start and end apart: 3 -> 0, of which waited for: 3 -> 0; matrix products, arithmetic and copies ran while one was open for 1% -> 0% of each run, Pallas kernels for 0% -> 0%
where the time goes in v1:
time: 96.6 us; the launch traced here: 96.4 us
  Pallas kernels  94.8 us (98%)
  local copies, waits for them, and re-layouts  1.54 us (2%)
    pallas_call x1, Pallas kernels, per_device(): pl.pallas_call(functools.partial(kernel, dims), out_shape=jax.ShapeDtypeS...  94.8 us

profile of v1, /device:TPU:1, one launch (start us, length us, event | category | flops | bytes accessed | tf_op | source)
XLA Modules:
  0.0 96.4 jit_solution(5940141108891457568)
XLA Ops:
  0.0 94.8 %mixer.1 = bf16[64,768]{1,0:T(8,128)(2,1)} custom-call(bf16[64,768]{1,0:T(8,128)(2,1)} %bitcast.12, bf16[32,64]{1,0:T(8,128)(2,1)} %refs_1_.1, f32[1,256]{1,0:T(1,128)} %bitcast.17, f32[1,256]{1,0:T(1,128)} %bitcast.18, bf16[64,256]{1,0:T(8,128)(2,1)} %bitcast.13, bf16[64,256]{1,0:T(8,128)(2,1)} %bitcast.14, bf16[64,256]{1,0:T(8,128)(2,1)} %bitcast.15, ...), custom_call_target="tpu_custom_call" | custom-call | tf_op jit(solution)/shard_map/mixer/pallas_call | solution.py:907
  94.8 1.5 %copy.19 = bf16[768,64]{0,1:T(8,128)(2,1)} copy(bf16[768,64]{0,1:T(8,128)(2,1)} %bitcast.11) | data formatting | bytes 196608

commit v2 on v1

--- a/solution.py
+++ b/solution.py
@@ -698,6 +698,8 @@
 
     mark("ctx_second")
     ctx_second()
+    mark("w_second")
+    w_second()
     mark("ctx_done")
     ctx_done()
     mark("zwait")
@@ -777,17 +779,17 @@
         r.acc2[...] = step if not ready2 else r.acc2[...] + step
         ready2.append(yy)
 
-    last_go2 = max([i for i, st in enumerate(plan2[2]) if st[1]], default=-1)
+    w_at = max([i for i, st in enumerate(plan2[2]) if st[1]], default=0)
     waiting2 = []
 
     def after2(s, when):
         if s < 0:
-            w_second()
             return
         waiting2.extend(done2[s])
-        if s == len(plan2[2]) - 1:
+        if s == w_at:
             with jax.named_scope("w_third"):
                 w_third()
+        if s >= w_at:
             while waiting2:
                 product(lax.rem(y - waiting2.pop(0) + Y, Y))
 

time: 96.6 us -> 94.2 us (0.975)
  Pallas kernels: 94.8 us -> 92.5 us
    pallas_call x1, Pallas kernels: 94.8 us -> 92.5 us  [per_device(): pl.pallas_call(functools.partial(kernel, dims), out_shape=jax.ShapeDtypeS...]
where the time goes in v2:
time: 94.2 us; the launch traced here: 94 us
  Pallas kernels  92.5 us (98%)
  local copies, waits for them, and re-layouts  1.54 us (2%)
    pallas_call x1, Pallas kernels, per_device(): pl.pallas_call(functools.partial(kernel, dims), out_shape=jax.ShapeDtypeS...  92.5 us

profile of v2, /device:TPU:1, one launch (start us, length us, event | category | flops | bytes accessed | tf_op | source)
XLA Modules:
  0.0 94.0 jit_solution(2877907355145321359)
XLA Ops:
  0.0 92.5 %mixer.1 = bf16[64,768]{1,0:T(8,128)(2,1)} custom-call(bf16[64,768]{1,0:T(8,128)(2,1)} %bitcast.12, bf16[32,64]{1,0:T(8,128)(2,1)} %refs_1_.1, f32[1,256]{1,0:T(1,128)} %bitcast.17, f32[1,256]{1,0:T(1,128)} %bitcast.18, bf16[64,256]{1,0:T(8,128)(2,1)} %bitcast.13, bf16[64,256]{1,0:T(8,128)(2,1)} %bitcast.14, bf16[64,256]{1,0:T(8,128)(2,1)} %bitcast.15, ...), custom_call_target="tpu_custom_call" | custom-call | tf_op jit(solution)/shard_map/mixer/pallas_call | solution.py:909
  92.5 1.5 %copy.19 = bf16[768,64]{0,1:T(8,128)(2,1)} copy(bf16[768,64]{0,1:T(8,128)(2,1)} %bitcast.11) | data formatting | bytes 196608
